TPU v7x, 32 devices: a whole 2x2x4 slice. The times are simulated.
32 devices in a mesh: sp: 8 (over z, y), tp: 4 (over x, core).
Axes of the slice: x: 2, y: 2, z: 4, core: 2. Of those that a mesh axis runs over, the one named last changes fastest.
Arguments:
- stream: bfloat16 [1536, 2048], P('sp'), may hold values from -6 to 6
- upstream: bfloat16 [1536, 2048], P('sp'), may hold values from -6 to 6
- expert_gain: float32 [2048], replicated, may hold values from 0.1 to 1.9
- expert_ids: int32 [1536, 2], P('sp'), may hold values from 0 to 7, all different within a row; in each aligned block of 192 rows (0 to 191, 192 to 383, ...) at most 60 rows name the same one
- group_weight: float32 [1536], P('sp'), may hold values from 0.25 to 1
- pair_scores: float32 [1536, 2], P('sp'), may hold values from -6 to 6
- gate_weight: bfloat16 [8, 2048, 1024], P('sp', None, 'tp'), may hold values from -0.125 to 0.125
- up_weight: bfloat16 [8, 2048, 1024], P('sp', None, 'tp'), may hold values from -0.125 to 0.125
- down_weight: bfloat16 [8, 1024, 2048], P('sp', 'tp'), may hold values from -0.1875 to 0.1875
- mixer_weight: bfloat16 [1024, 2048], P('tp'), may hold values from -0.1875 to 0.1875
- filtered: bfloat16 [1536, 1024], P('sp', 'tp'), may hold values from -1000 to 1000
- channel_gain: float32 [1024], P('tp'), may hold values from 0.1 to 1.9
- kernel_taps: float32 [31, 1024], P(None, 'tp'), may hold values from -1 to 1
- value_branch: bfloat16 [1536, 1024], P('sp', 'tp'), may hold values from -6 to 6
- gate_branch: bfloat16 [1536, 1024], P('sp', 'tp'), may hold values from -6 to 6
Outputs:
- gradient_value: bfloat16 [1536, 1024], P('sp', 'tp')
- gradient_gating: bfloat16 [1536, 1024], P('sp', 'tp')
- gradient_mixer: float32 [2048, 1024], P('sp', 'tp')
- gradient_gate: float32 [8, 2048, 1024], P('sp', None, 'tp')
- gradient_up: float32 [8, 2048, 1024], P('sp', None, 'tp')
- gradient_down: float32 [8, 1024, 2048], P('sp', 'tp')
Inputs may be any that keep to these rules, and one draw needn't show every extreme that they name: `expert_ids`: the two experts of a token differ. Among the rows of one index of sp, at most 60 routes name the same expert, and in every draw some expert is named by exactly 60 of them.
All inputs are finite; a program needn't handle non-finite values.
Results may differ from a plain program's by a relative error of at most 0.012.
Values may be sent and summed in bfloat16 or wider, within the bound.
No kernel may reach another device: no remote copies, remote signals or barrier semaphores. Data moves between devices by JAX's collectives and lax.ppermute only.
A program may use at most 64 MiB of HBM per device.

v0:
```python
import jax
import jax.numpy as jnp
from jax import lax
from jax.sharding import PartitionSpec as P

EPS = 1e-06


def shifted(block, axis, distance):
    devices = range(lax.axis_size(axis))
    route = [(i - distance, i) for i in devices if i - distance in devices]
    return lax.ppermute(block, axis, route)


def route_slots(routes, capacity, experts):
    flat = routes.reshape(-1)
    onehot = (flat[:, None] == jnp.arange(experts, dtype=jnp.int32)[None, :]).astype(jnp.int32)
    before = jnp.cumsum(onehot, axis=0) - onehot
    position = jnp.sum(before * onehot, axis=1)
    slots = flat * capacity + position
    total = flat.shape[0]
    source = (
        jnp.full((experts * capacity,), total, jnp.int32)
        .at[slots]
        .set(jnp.arange(total, dtype=jnp.int32))
    )
    return (slots, source)


def silu_slope(value, sigma):
    return sigma * (1.0 + value * (1.0 - sigma))


def pack_routes(normed, scaled, source, experts, capacity):
    total = scaled.shape[0]
    token_index = jnp.where(source < total, source // 2, normed.shape[0])
    normed_ext = jnp.concatenate([normed, jnp.zeros((1, normed.shape[1]), normed.dtype)], axis=0)
    scaled_ext = jnp.concatenate([scaled, jnp.zeros((1, scaled.shape[1]), scaled.dtype)], axis=0)
    return (
        normed_ext[token_index].reshape(experts, capacity, -1),
        scaled_ext[source].reshape(experts, capacity, -1),
    )


def contract_last(left, right):
    return lax.dot_general(
        left, right, (((1,), (1,)), ((), ())), preferred_element_type=jnp.float32
    )


def contract_first(left, right):
    return lax.dot_general(
        left, right, (((0,), (0,)), ((), ())), preferred_element_type=jnp.float32
    )


def body(
    stream,
    upstream,
    expert_gain,
    expert_ids,
    group_weight,
    pair_scores,
    gate_weight,
    up_weight,
    down_weight,
    mixer_weight,
    filtered,
    channel_gain,
    kernel_taps,
    value_branch,
    gate_branch,
):
    experts = lax.axis_size("sp")
    tokens_here, width = stream.shape
    capacity = max(2, 5 * tokens_here // (2 * experts))
    groups = lax.axis_size("tp")
    column = width // groups
    first_col = lax.axis_index("tp") * column
    stream_f = stream.astype(jnp.float32)
    inv_rms = lax.rsqrt(jnp.mean(stream_f * stream_f, axis=1, keepdims=True) + EPS)
    normed = (stream_f * inv_rms * expert_gain).astype(jnp.bfloat16)
    spread = pair_scores[:, 0] - pair_scores[:, 1]
    route_weight = group_weight[:, None] * jnp.stack(
        [jax.nn.sigmoid(spread), jax.nn.sigmoid(-spread)], axis=1
    )
    scaled = (
        (route_weight[:, :, None] * upstream.astype(jnp.float32)[:, None, :])
        .astype(jnp.bfloat16)
        .reshape(2 * tokens_here, width)
    )
    slots, source = route_slots(expert_ids, capacity, experts)
    normed_part = lax.dynamic_slice_in_dim(normed, first_col, column, 1)
    scaled_part = lax.dynamic_slice_in_dim(scaled, first_col, column, 1)
    send_rows, send_cots = pack_routes(normed_part, scaled_part, source, experts, capacity)
    got_rows, got_cots = (
        lax.all_to_all(send_rows, "sp", split_axis=0, concat_axis=0, tiled=True),
        lax.all_to_all(send_cots, "sp", split_axis=0, concat_axis=0, tiled=True),
    )
    got_rows, got_cots = (
        lax.all_gather(got_rows, "tp", axis=2, tiled=True),
        lax.all_gather(got_cots, "tp", axis=2, tiled=True),
    )
    rows = got_rows.reshape(experts * capacity, width)
    cots = got_cots.reshape(experts * capacity, width)
    gate_local = gate_weight[0]
    up_local = up_weight[0]
    down_local = down_weight[0]
    pre_gate = jnp.dot(rows, gate_local, preferred_element_type=jnp.float32)
    pre_up = jnp.dot(rows, up_local, preferred_element_type=jnp.float32)
    sigma = jax.nn.sigmoid(pre_gate)
    silu_gate = pre_gate * sigma
    hidden = (silu_gate * pre_up).astype(jnp.bfloat16)
    grad_hidden = contract_last(cots, down_local)
    grad_pre_gate = (grad_hidden * pre_up * silu_slope(pre_gate, sigma)).astype(jnp.bfloat16)
    grad_pre_up = (grad_hidden * silu_gate).astype(jnp.bfloat16)
    partial_rows = contract_last(grad_pre_gate, gate_local) + contract_last(grad_pre_up, up_local)
    shared = lax.psum_scatter(
        partial_rows.astype(jnp.bfloat16), "tp", scatter_dimension=1, tiled=True
    )
    back = lax.all_to_all(
        shared.reshape(experts, capacity, column), "sp", split_axis=0, concat_axis=0, tiled=True
    )
    back = lax.all_gather(back, "tp", axis=2, tiled=True)
    gradient_gate = contract_first(rows, grad_pre_gate)[None]
    gradient_up = contract_first(rows, grad_pre_up)[None]
    gradient_down = contract_first(hidden, cots)[None]
    back_flat = back.reshape(experts * capacity, width)
    per_route = back_flat[slots].astype(jnp.float32).reshape(tokens_here, 2, width)
    grad_normed = per_route[:, 0] + per_route[:, 1]
    weighted = grad_normed * expert_gain
    inner = jnp.mean(weighted * stream_f, axis=1, keepdims=True)
    grad_stream = (
        upstream.astype(jnp.float32)
        + inv_rms * weighted
        - stream_f * inv_rms * inv_rms * inv_rms * inner
    ).astype(jnp.bfloat16)
    grad_act = contract_last(grad_stream, mixer_weight)
    filt = filtered.astype(jnp.float32)
    channels = filt.shape[1] * groups
    total_sum, total_square = lax.psum((jnp.sum(filt, axis=1), jnp.sum(filt * filt, axis=1)), "tp")
    mean_c = total_sum[:, None] / channels
    variance = total_square[:, None] / channels - mean_c * mean_c
    inv_std = lax.rsqrt(variance + EPS)
    centred = (filt - mean_c) * inv_std
    normal_out = centred * channel_gain
    sig_norm = jax.nn.sigmoid(normal_out)
    activated = (normal_out * sig_norm).astype(jnp.bfloat16)
    grad_centred = grad_act * silu_slope(normal_out, sig_norm) * channel_gain
    slope_sum, slope_cross = lax.psum(
        (jnp.sum(grad_centred, axis=1), jnp.sum(grad_centred * centred, axis=1)), "tp"
    )
    grad_filtered = (
        inv_std
        * (grad_centred - slope_sum[:, None] / channels - centred * slope_cross[:, None] / channels)
    ).astype(jnp.bfloat16)
    reach = kernel_taps.shape[0] - 1
    ahead = shifted(grad_filtered[:reach], "sp", -1)
    extended = jnp.concatenate([grad_filtered, ahead], axis=0).astype(jnp.float32)
    grad_mixed = lax.conv_general_dilated(
        extended[None],
        kernel_taps[::-1][:, None, :],
        (1,),
        "VALID",
        dimension_numbers=("NWC", "WIO", "NWC"),
        feature_group_count=filt.shape[1],
        precision=lax.Precision.HIGHEST,
    )[0]
    sig_gate = jax.nn.sigmoid(gate_branch.astype(jnp.float32))
    gradient_value = (grad_mixed * sig_gate).astype(jnp.bfloat16)
    gradient_gating = (
        grad_mixed * value_branch.astype(jnp.float32) * sig_gate * (1.0 - sig_gate)
    ).astype(jnp.bfloat16)
    gradient_mixer = lax.psum_scatter(
        contract_first(grad_stream, activated), "sp", scatter_dimension=0, tiled=True
    )
    return (
        gradient_value,
        gradient_gating,
        gradient_mixer,
        gradient_gate,
        gradient_up,
        gradient_down,
    )


def solution(mesh):
    return jax.shard_map(
        body,
        mesh=mesh,
        in_specs=(
            P("sp", None),
            P("sp", None),
            P(),
            P("sp", None),
            P("sp"),
            P("sp", None),
            P("sp", None, "tp"),
            P("sp", None, "tp"),
            P("sp", "tp", None),
            P("tp", None),
            P("sp", "tp"),
            P("tp"),
            P(None, "tp"),
            P("sp", "tp"),
            P("sp", "tp"),
        ),
        out_specs=(
            P("sp", "tp"),
            P("sp", "tp"),
            P("sp", "tp"),
            P("sp", None, "tp"),
            P("sp", None, "tp"),
            P("sp", "tp", None),
        ),
        check_vma=False,
    )
```

profile of v0, /device:TPU:0, one launch (start us, length us, event | category | flops | bytes accessed | tf_op | source)
XLA Modules:
  0.0 268.8 jit_solution(1533650336860865618)
XLA Ops:
  7.2 0.9 copy.25
  8.1 0.1 eq.29
  8.3 0.1 eq.25
  8.4 0.7 broadcast_multiply_fusion
  9.1 1.4 fusion
  10.5 1.3 convert_multiply_fusion.1
  11.8 0.9 reduce-window.6
  12.7 0.2 slice_reduce_fusion
  12.9 0.1 copy.24
  13.1 0.1 mul.216
  13.2 0.1 fusion.51
  13.3 2.9 %scatter_custom_fusion = s32[480]{0:T(512)S(1)} fusion(s32[384]{0:T(512)S(1)} %fusion.56, s32[384]{0:T(512)S(1)} %iota.11, s32[]{:T(128)} %constant.56.clone.1), kind=kCustom, calls=%fused_computation.99 | custom fusion | bytes 1924 | tf_op jit(solution)/shard_map/scatter | solution.py:25
  16.3 0.1 dynamic-slice
  16.4 2.1 gather_fusion.1
  18.6 0.1 reshape.138
  18.7 21.9 %all_to_all.15 = bf16[8,60,512]{2,1,0:T(8,128)(2,1)} all-to-all(bf16[8,60,512]{2,1,0:T(8,128)(2,1)S(1)} %reshape.138), channel_id=1, replica_groups=mesh['sp'=8,'tp'=4] {'sp'}, dimensions={0} | all-to-all | bytes 983040 | tf_op jit(solution)/shard_map/all_to_all | solution.py:97
  40.6 0.0 all-gather.4.cloned.1.call-start
  40.7 0.1 copy.23
  40.8 0.1 stack.14
  41.0 0.1 mul.206
  41.1 0.1 mul.207
  41.2 3.2 %mul.210 = f32[192,2,2048]{2,1,0:T(2,128)} broadcast(bf16[192,2048]{1,0:T(8,128)(2,1)S(1)} %copy-done.4), dimensions={0,2} | broadcast | bytes 3932160 | tf_op jit(solution)/shard_map/mul | solution.py:88
  44.5 5.6 %mul.211 = f32[384,2048]{1,0:T(8,128)} reshape(f32[192,2,2048]{2,1,0:T(2,128)} %mul.210) | data formatting | bytes 6291456 | tf_op jit(solution)/shard_map/mul | solution.py:88
  50.1 1.2 fusion.14
  51.4 2.1 gather_fusion
  53.5 0.1 reshape.136
  53.6 17.4 %all_to_all.16 = bf16[8,60,512]{2,1,0:T(8,128)(2,1)} all-to-all(bf16[8,60,512]{2,1,0:T(8,128)(2,1)S(1)} %reshape.136), channel_id=1, replica_groups=mesh['sp'=8,'tp'=4] {'sp'}, dimensions={0} | all-to-all | bytes 983040 | tf_op jit(solution)/shard_map/all_to_all | solution.py:98
  71.0 0.0 reduce-scatter.3.cloned.1.call-start
  71.0 1.7 reshape.139
  72.8 2.6 fusion.10
  75.4 1.5 fusion.7
  76.9 15.8 %all-gather.4.cloned.1.call-done = bf16[8,60,2048]{2,1,0:T(8,128)(2,1)} async-done(((bf16[8,60,512]{2,1,0:T(8,128)(2,1)}), bf16[8,60,2048]{2,1,0:T(8,128)(2,1)}) %all-gather.4.cloned.1.call-update) | async-done | bytes 1966096 | tf_op jit(solution)/shard_map/all_gather | solution.py:102
  92.7 1.7 reshape.137
  94.5 2.8 %multiply_convert_fusion.1 = (bf16[480,256]{1,0:T(8,128)(2,1)S(1)}, bf16[480,256]{1,0:T(8,128)(2,1)S(1)}) fusion(f32[480,256]{1,0:T(8,128)} %fusion.7, f32[480,256]{1,0:T(8,128)S(1)} %fusion.10, bf16[480,2048]{1,0:T(8,128)(2,1)S(1)} %reshape.137, bf16[1,256,2048]{2,1,0:T(8,128)(2,1)} %param.23), kind=kOutput, calls=%fused_computation.31 | convolution fusion | flops 504913920 | bytes 4489216 | tf_op jit(solution)/shard_map/dot_general | solution.py:46
  97.4 0.7 fusion.5
  98.1 0.6 copy-done.7
  98.8 2.0 add_convert_fusion
  100.8 0.0 all-gather.8.cloned.1.call-start
  100.8 30.5 %reduce-scatter.3.cloned.1.call-done = bf16[480,512]{1,0:T(8,128)(2,1)} async-done(((bf16[480,2048]{1,0:T(8,128)(2,1)}), bf16[480,512]{1,0:T(8,128)(2,1)}) %reduce-scatter.3.cloned.1.call-update) | async-done | bytes 491536 | tf_op jit(solution)/shard_map/reduce_scatter | solution.py:118
  131.3 1.1 reshape.140
  132.4 19.8 %all_to_all.17 = bf16[8,60,512]{2,1,0:T(8,128)(2,1)} all-to-all(bf16[8,60,512]{2,1,0:T(8,128)(2,1)S(1)} %reshape.140), channel_id=1, replica_groups=mesh['sp'=8,'tp'=4] {'sp'}, dimensions={0} | all-to-all | bytes 983040 | tf_op jit(solution)/shard_map/all_to_all | solution.py:121
  152.3 0.2 fusion.19
  152.5 6.1 %all-reduce.3 = (f32[192]{0:T(256)S(1)}, f32[192]{0:T(256)S(1)}) all-reduce(f32[192]{0:T(256)S(1)} %get-tuple-element.9, f32[192]{0:T(256)S(1)} %get-tuple-element.8), channel_id=1, replica_groups=mesh['sp'=8,'tp'=4] {'tp'}, use_global_device_ids=true, to_apply=%region_3.4 | all-reduce | flops 384 | bytes 3072 | tf_op jit(solution)/shard_map/psum | solution.py:141
  158.6 14.4 %all-gather.8.cloned.1.call-done = bf16[8,60,2048]{2,1,0:T(8,128)(2,1)} async-done(((bf16[8,60,512]{2,1,0:T(8,128)(2,1)}), bf16[8,60,2048]{2,1,0:T(8,128)(2,1)}) %all-gather.8.cloned.1.call-update) | async-done | bytes 1966096 | tf_op jit(solution)/shard_map/all_gather | solution.py:124
  173.0 1.7 reshape.141
  174.8 3.1 %gather_fusion.2 = bf16[384,2048]{1,0:T(8,128)(2,1)} fusion(bf16[480,2048]{1,0:T(8,128)(2,1)S(1)} %reshape.141, s32[1024]{0:T(1024)S(1)} %pad_clamp_fusion), kind=kCustom, calls=%fused_computation.2 | custom fusion | bytes 3147264 | tf_op jit(solution)/shard_map/gather | solution.py:129
  177.9 4.7 %reshape.142 = f32[192,2,2048]{2,1,0:T(2,128)} reshape(bf16[384,2048]{1,0:T(8,128)(2,1)} %gather_fusion.2) | data formatting | bytes 4718592 | tf_op jit(solution)/shard_map/convert_element_type | solution.py:129
  182.6 6.1 %fusion.62 = (f32[192,1,2048]{2,1,0:T(1,128)S(1)}, f32[192,1,2048]{2,1,0:T(1,128)S(1)}) fusion(f32[192,2,2048]{2,1,0:T(2,128)} %reshape.142), kind=kLoop, calls=%fused_computation.112 | loop fusion | bytes 6291456 | tf_op jit(solution)/shard_map/slice | solution.py:130
  188.8 1.0 fusion.1
  189.8 0.1 copy-done.5
  189.9 1.9 subtract_convert_fusion
  191.8 1.9 fusion.42
  193.8 0.1 rev.3
  193.9 3.8 %convolution_bitcast_fusion.1 = f32[1,2048,256]{2,1,0:T(8,128)} fusion(bf16[480,2048]{1,0:T(8,128)(2,1)} %copy-done.6, bf16[480,256]{1,0:T(8,128)(2,1)S(1)} %copy-done.13), kind=kOutput, calls=%fused_computation.6 | convolution fusion | flops 503316480 | bytes 4308992 | tf_op jit(solution)/shard_map/dot_general | solution.py:52
  197.7 2.1 convolution_bitcast_fusion
  199.8 0.6 fusion.61
  200.5 6.3 %all-reduce.2 = (f32[192]{0:T(256)S(1)}, f32[192]{0:T(256)S(1)}) all-reduce(f32[192]{0:T(256)S(1)} %get-tuple-element.7, f32[192]{0:T(256)S(1)} %get-tuple-element.6), channel_id=1, replica_groups=mesh['sp'=8,'tp'=4] {'tp'}, use_global_device_ids=true, to_apply=%region_14.15 | all-reduce | flops 384 | bytes 3072 | tf_op jit(solution)/shard_map/psum | solution.py:150
  206.8 0.2 fusion.37
  206.9 1.3 collective-permute-start
  208.3 3.6 %convolution_bitcast_fusion.2 = f32[1,2048,256]{2,1,0:T(8,128)} fusion(bf16[480,2048]{1,0:T(8,128)(2,1)} %copy-done.6, bf16[480,256]{1,0:T(8,128)(2,1)S(1)} %copy-done.15), kind=kOutput, calls=%fused_computation.7 | convolution fusion | flops 503316480 | bytes 4308992 | tf_op jit(solution)/shard_map/dot_general | solution.py:52
  211.9 0.7 collective-permute-done
  212.6 2.9 %fusion.17 = f32[1,192,256]{2,0,1:T(1,128)S(1)} fusion(bf16[1,222,256]{2,1,0:T(8,128)(2,1)S(1)} %maximum_bitcast_fusion, f32[31,1,256]{2,0,1:T(8,128)S(1)} %bitcast.71), kind=kOutput, calls=%fused_computation.40 | convolution fusion | flops 18284544 | bytes 342016 | tf_op jit(solution)/shard_map/conv_general_dilated | solution.py:160
  215.5 0.8 fusion.41
  216.2 46.0 %reduce-scatter.5.cloned.1.call-done = f32[256,256]{1,0:T(8,128)} async-done(((f32[2048,256]{1,0:T(8,128)}), f32[256,256]{1,0:T(8,128)}) %reduce-scatter.5.cloned.1.call-update) | async-done | bytes 262160 | tf_op jit(solution)/shard_map/reduce_scatter | solution.py:174
  (74 shorter events, 0.6 us)
Async XLA Ops:
  7.2 68.3 %copy-start = (bf16[1,2048,256]{2,1,0:T(8,128)(2,1)S(1)}, bf16[1,2048,256]{2,1,0:T(8,128)(2,1)}, u32[]{:S(2)}) copy-start(bf16[1,2048,256]{2,1,0:T(8,128)(2,1)} %param.21) | copy-start | bytes 3145732
  7.2 9.1 %copy-start.18 = (f32[2048]{0:T(1024)S(1)}, f32[2048]{0:T(1024)}, u32[]{:S(2)}) copy-start(f32[2048]{0:T(1024)} %param.17) | copy-start | bytes 24580
  7.2 63.8 %all-gather.6.cloned.1.call-start = ((), (), s32[]{:S(2)}) async-start(), calls=%async_computation.6 | async-start | bytes 2621440 | tf_op jit(solution)/shard_map/all_gather | solution.py:101
  18.6 22.1 %copy-start.20 = (f32[192,2]{0,1:T(2,128)S(1)}, f32[192,2]{0,1:T(2,128)}, u32[]{:S(2)}) copy-start(f32[192,2]{0,1:T(2,128)} %param.20) | copy-start | bytes 4612
  18.6 22.4 %copy-start.21 = (f32[192]{0:T(256)S(1)}, f32[192]{0:T(256)}, u32[]{:S(2)}) copy-start(f32[192]{0:T(256)} %param.19) | copy-start | bytes 2308
  18.6 22.6 %copy-start.4 = (bf16[192,2048]{1,0:T(8,128)(2,1)S(1)}, bf16[192,2048]{1,0:T(8,128)(2,1)}, u32[]{:S(2)}) copy-start(bf16[192,2048]{1,0:T(8,128)(2,1)} %param.16) | copy-start | bytes 2359300
  40.6 52.1 %all-gather.4.cloned.1.call-start = ((), (), s32[]{:S(2)}) async-start(), calls=%async_computation.5 | async-start | bytes 2621440 | tf_op jit(solution)/shard_map/all_gather | solution.py:102
  71.0 60.4 %reduce-scatter.3.cloned.1.call-start = ((), (), s32[]{:S(2)}) async-start(), calls=%async_computation.7 | async-start | bytes 2457600 | tf_op jit(solution)/shard_map/reduce_scatter | solution.py:118
  72.8 4.1 %copy-start.6 = (bf16[480,2048]{1,0:T(8,128)(2,1)}, bf16[480,2048]{1,0:T(8,128)(2,1)S(1)}, u32[]{:S(2)}) copy-start(bf16[480,2048]{1,0:T(8,128)(2,1)S(1)} %reshape.139) | copy-start | bytes 5898244
  75.4 19.1 %copy-start.9 = (f32[480,256]{1,0:T(8,128)}, f32[480,256]{1,0:T(8,128)S(1)}, u32[]{:S(2)}) copy-start(f32[480,256]{1,0:T(8,128)S(1)} %fusion.10) | copy-start | bytes 1474564
  94.5 2.8 %copy-start.2 = (bf16[480,2048]{1,0:T(8,128)(2,1)}, bf16[480,2048]{1,0:T(8,128)(2,1)S(1)}, u32[]{:S(2)}) copy-start(bf16[480,2048]{1,0:T(8,128)(2,1)S(1)} %reshape.137) | copy-start | bytes 5898244
  97.4 0.8 copy-start.14
  97.4 0.8 copy-start.12
  97.4 1.4 copy-start.7
  100.8 51.5 %copy-start.8 = (bf16[192,256]{1,0:T(8,128)(2,1)S(1)}, bf16[192,256]{1,0:T(8,128)(2,1)}, u32[]{:S(2)}) copy-start(bf16[192,256]{1,0:T(8,128)(2,1)} %param.25) | copy-start | bytes 294916
  100.8 72.3 %all-gather.8.cloned.1.call-start = ((), (), s32[]{:S(2)}) async-start(), calls=%async_computation.8 | async-start | bytes 2621440 | tf_op jit(solution)/shard_map/all_gather | solution.py:124
  152.3 110.0 %reduce-scatter.5.cloned.1.call-start = ((), (), s32[]{:S(2)}) async-start(), calls=%async_computation.9 | async-start | bytes 2359296 | tf_op jit(solution)/shard_map/reduce_scatter | solution.py:174
  182.6 6.1 %copy-start.1 = (bf16[192,2048]{1,0:T(8,128)(2,1)S(1)}, bf16[192,2048]{1,0:T(8,128)(2,1)}, u32[]{:S(2)}) copy-start(bf16[192,2048]{1,0:T(8,128)(2,1)} %param.15) | copy-start | bytes 2359300
  188.8 1.1 copy-start.5
  189.9 1.9 copy-start.22
  191.8 1.9 copy-start.19
  191.8 2.0 copy-start.13
  193.9 3.8 %copy-start.3 = (bf16[480,2048]{1,0:T(8,128)(2,1)S(1)}, bf16[480,2048]{1,0:T(8,128)(2,1)}, u32[]{:S(2)}) copy-start(bf16[480,2048]{1,0:T(8,128)(2,1)} %copy-done.2) | copy-start | bytes 5898244
  193.9 3.8 %copy-start.10 = (f32[480,256]{1,0:T(8,128)S(1)}, f32[480,256]{1,0:T(8,128)}, u32[]{:S(2)}) copy-start(f32[480,256]{1,0:T(8,128)} %copy-done.9) | copy-start | bytes 1474564
  193.9 3.8 %copy-start.11 = (f32[480,256]{1,0:T(8,128)S(1)}, f32[480,256]{1,0:T(8,128)}, u32[]{:S(2)}) copy-start(f32[480,256]{1,0:T(8,128)} %fusion.7) | copy-start | bytes 1474564
  197.7 2.1 copy-start.23
  199.8 8.4 %copy-start.15 = (bf16[480,256]{1,0:T(8,128)(2,1)S(1)}, bf16[480,256]{1,0:T(8,128)(2,1)}, u32[]{:S(2)}) copy-start(bf16[480,256]{1,0:T(8,128)(2,1)} %copy-done.14) | copy-start | bytes 737284
  206.9 5.6 %collective-permute-start = (bf16[30,256]{1,0:T(8,128)(2,1)S(1)}, bf16[30,256]{1,0:T(8,128)(2,1)S(1)}, u32[]{:S(2)}, u32[]{:S(2)}) collective-permute-start(bf16[30,256]{1,0:T(8,128)(2,1)S(1)} %slice.37), channel_id=1, source_target_pairs={{4,0},{8,4},{12,8},{16,12},{20,16},{24,20},{28,24},{5,1},{9,5},{13... | collective-permute-start | bytes 46088 | tf_op jit(solution)/shard_map/ppermute | solution.py:12
  212.6 2.9 %copy-start.16 = (bf16[192,256]{1,0:T(8,128)(2,1)S(1)}, bf16[192,256]{1,0:T(8,128)(2,1)}, u32[]{:S(2)}) copy-start(bf16[192,256]{1,0:T(8,128)(2,1)} %param.28) | copy-start | bytes 294916
  212.6 2.9 %copy-start.17 = (bf16[192,256]{1,0:T(8,128)(2,1)S(1)}, bf16[192,256]{1,0:T(8,128)(2,1)}, u32[]{:S(2)}) copy-start(bf16[192,256]{1,0:T(8,128)(2,1)} %param.29) | copy-start | bytes 294916
Sparse Core Ops, SparseCore 0:
  40.7 21.5 all-gather.5
  71.1 21.6 all-gather.3
  100.9 30.3 reduce-scatter.2
  152.4 20.6 all-gather.7
  193.9 68.3 reduce-scatter.4
where the time goes:
time: 270 us; the launch traced here: 269 us
  waiting for transfers between devices  108 us (40%)
  blocking collectives  71.4 us (26%)
  local copies, waits for them, and re-layouts  39.8 us (15%)
  matrix products  24.5 us (9%)
  between operations  14.4 us (5%)
  other arithmetic  9.69 us (4%)
    reduce_scatter x1, waiting for transfers between devices, body(): lax.psum_scatter(contract_first(grad_stream, activated), 'sp', scatter_di...  46 us
    reduce_scatter x1, waiting for transfers between devices, body(): lax.psum_scatter(partial_rows.astype(jnp.bfloat16), 'tp', scatter_dimensi...  30.5 us
    all_to_all x1, blocking collectives, body(): lax.all_to_all(send_rows, 'sp', split_axis=0, concat_axis=0, tiled=True)  21.9 us
    all_to_all x1, blocking collectives, body(): lax.all_to_all(shared.reshape(experts, capacity, column), 'sp', split_axi...  19.8 us
    all_to_all x1, blocking collectives, body(): lax.all_to_all(send_cots, 'sp', split_axis=0, concat_axis=0, tiled=True)  17.4 us
    all_gather x1, waiting for transfers between devices, body(): lax.all_gather(got_cots, 'tp', axis=2, tiled=True)  15.8 us
    all_gather x1, waiting for transfers between devices, body(): back = lax.all_gather(back, 'tp', axis=2, tiled=True)  14.4 us
    dot_general x4, matrix products, contract_first(): lax.dot_general(left, right, (((0,), (0,)), ((), ())), preferred_element_...  11.4 us
  transfers between devices with their start and end apart: 6, of which 5 were waited for; matrix products, arithmetic and copies ran while one was open for 12% of the time, Pallas kernels for 0%

commit v1 on v0

--- a/solution.py
+++ b/solution.py
@@ -1,9 +1,26 @@
+import functools
 import jax
 import jax.numpy as jnp
 from jax import lax
 from jax.sharding import PartitionSpec as P
 
 EPS = 1e-06
+
+
+def draw_panels(v0, named_axis):
+    size_here = lax.psum(1, axis_name=named_axis)
+    part_next = sorted(((to_i, (to_i + 1) % size_here) for to_i in range(size_here)))
+    then = v0
+    ledger = [then]
+    for kk in tuple(range(1, size_here)):
+        then = lax.ppermute(then, named_axis, perm=part_next)
+        ledger.insert(0, then)
+    z = jnp.concatenate(ledger, axis=2)
+    z_new = lax.axis_index(named_axis)
+    return jnp.roll(z, (z_new + 1) * v0.shape[2], axis=2)
+
+
+link_flows = functools.partial(draw_panels, named_axis="tp")
 
 
 def shifted(block, axis, distance):
@@ -121,7 +138,7 @@
     back = lax.all_to_all(
         shared.reshape(experts, capacity, column), "sp", split_axis=0, concat_axis=0, tiled=True
     )
-    back = lax.all_gather(back, "tp", axis=2, tiled=True)
+    back = link_flows(back)
     gradient_gate = contract_first(rows, grad_pre_gate)[None]
     gradient_up = contract_first(rows, grad_pre_up)[None]
     gradient_down = contract_first(hidden, cots)[None]

time: 270 us -> 276 us (1.022)
  blocking collectives: 71.4 us -> 74.5 us
    ppermute x0 -> x3, waiting for transfers between devices: none -> 17.2 us  [draw_panels(): then = lax.ppermute(then, named_axis, perm=part_next)]
    all_gather x1 -> x0, waiting for transfers between devices: 14.4 us -> none  [body(): back = lax.all_gather(back, 'tp', axis=2, tiled=True)]
    psum x1, blocking collectives: 6.12 us -> 9.38 us  [body(): lax.psum((jnp.sum(filt, axis=1), jnp.sum(filt * filt, axis=1)), 'tp')]
  transfers between devices with their start and end apart: 6 -> 8, of which waited for: 5 -> 6; matrix products, arithmetic and copies ran while one was open for 12% -> 12% of each run, Pallas kernels for 0% -> 0%
where the time goes in v1:
time: 276 us; the launch traced here: 275 us
  waiting for transfers between devices  108 us (39%)
  blocking collectives  74.5 us (27%)
  local copies, waits for them, and re-layouts  41.9 us (15%)
  matrix products  24.5 us (9%)
  between operations  14.4 us (5%)
  other arithmetic  9.69 us (4%)
    reduce_scatter x1, waiting for transfers between devices, body(): lax.psum_scatter(contract_first(grad_stream, activated), 'sp', scatter_di...  44 us
    reduce_scatter x1, waiting for transfers between devices, body(): lax.psum_scatter(partial_rows.astype(jnp.bfloat16), 'tp', scatter_dimensi...  30.5 us
    all_to_all x1, blocking collectives, body(): lax.all_to_all(send_rows, 'sp', split_axis=0, concat_axis=0, tiled=True)  21.9 us
    all_to_all x1, blocking collectives, body(): lax.all_to_all(shared.reshape(experts, capacity, column), 'sp', split_axi...  19.7 us
    all_to_all x1, blocking collectives, body(): lax.all_to_all(send_cots, 'sp', split_axis=0, concat_axis=0, tiled=True)  17.4 us
    ppermute x3, waiting for transfers between devices, draw_panels(): then = lax.ppermute(then, named_axis, perm=part_next)  17.2 us
    all_gather x1, waiting for transfers between devices, body(): lax.all_gather(got_cots, 'tp', axis=2, tiled=True)  15.8 us
    dot_general x4, matrix products, contract_first(): lax.dot_general(left, right, (((0,), (0,)), ((), ())), preferred_element_...  11.5 us
  transfers between devices with their start and end apart: 8, of which 6 were waited for; matrix products, arithmetic and copies ran while one was open for 12% of the time, Pallas kernels for 0%

profile of v1, /device:TPU:0, one launch (start us, length us, event | category | flops | bytes accessed | tf_op | source)
XLA Modules:
  0.0 274.9 jit_solution(9423651058188426807)
XLA Ops:
  7.2 0.9 copy.25
  8.1 0.1 eq.32
  8.3 0.1 eq.28
  8.4 0.7 broadcast_multiply_fusion
  9.1 1.4 fusion
  10.5 1.3 convert_multiply_fusion.1
  11.8 0.9 reduce-window.6
  12.7 0.2 slice_reduce_fusion
  12.9 0.1 copy.24
  13.1 0.1 mul.219
  13.2 0.1 fusion.51
  13.3 2.9 %scatter_custom_fusion = s32[480]{0:T(512)S(1)} fusion(s32[384]{0:T(512)S(1)} %fusion.56, s32[384]{0:T(512)S(1)} %iota.11, s32[]{:T(128)} %constant.75.clone.1), kind=kCustom, calls=%fused_computation.107 | custom fusion | bytes 1924 | tf_op jit(solution)/shard_map/scatter | solution.py:42
  16.3 0.1 dynamic-slice
  16.4 2.1 gather_fusion.1
  18.6 0.1 reshape.138
  18.7 21.9 %all_to_all.15 = bf16[8,60,512]{2,1,0:T(8,128)(2,1)} all-to-all(bf16[8,60,512]{2,1,0:T(8,128)(2,1)S(1)} %reshape.138), channel_id=1, replica_groups=mesh['sp'=8,'tp'=4] {'sp'}, dimensions={0} | all-to-all | bytes 983040 | tf_op jit(solution)/shard_map/all_to_all | solution.py:114
  40.7 0.1 copy.23
  40.8 0.1 stack.14
  41.0 0.1 mul.209
  41.1 0.1 mul.210
  41.2 3.2 %mul.213 = f32[192,2,2048]{2,1,0:T(2,128)} broadcast(bf16[192,2048]{1,0:T(8,128)(2,1)S(1)} %copy-done.4), dimensions={0,2} | broadcast | bytes 3932160 | tf_op jit(solution)/shard_map/mul | solution.py:105
  44.5 5.6 %mul.214 = f32[384,2048]{1,0:T(8,128)} reshape(f32[192,2,2048]{2,1,0:T(2,128)} %mul.213) | data formatting | bytes 6291456 | tf_op jit(solution)/shard_map/mul | solution.py:105
  50.1 1.2 fusion.14
  51.4 2.1 gather_fusion
  53.5 0.1 reshape.136
  53.6 17.4 %all_to_all.16 = bf16[8,60,512]{2,1,0:T(8,128)(2,1)} all-to-all(bf16[8,60,512]{2,1,0:T(8,128)(2,1)S(1)} %reshape.136), channel_id=1, replica_groups=mesh['sp'=8,'tp'=4] {'sp'}, dimensions={0} | all-to-all | bytes 983040 | tf_op jit(solution)/shard_map/all_to_all | solution.py:115
  71.0 1.7 reshape.139
  72.8 2.6 fusion.10
  75.4 1.5 fusion.7
  76.9 15.8 %all-gather.3.cloned.1.call-done = bf16[8,60,2048]{2,1,0:T(8,128)(2,1)} async-done(((bf16[8,60,512]{2,1,0:T(8,128)(2,1)}), bf16[8,60,2048]{2,1,0:T(8,128)(2,1)}) %all-gather.3.cloned.1.call-update) | async-done | bytes 1966096 | tf_op jit(solution)/shard_map/all_gather | solution.py:119
  92.7 1.7 reshape.137
  94.5 2.8 %multiply_convert_fusion.1 = (bf16[480,256]{1,0:T(8,128)(2,1)S(1)}, bf16[480,256]{1,0:T(8,128)(2,1)S(1)}) fusion(f32[480,256]{1,0:T(8,128)} %fusion.7, f32[480,256]{1,0:T(8,128)S(1)} %fusion.10, bf16[480,2048]{1,0:T(8,128)(2,1)S(1)} %reshape.137, bf16[1,256,2048]{2,1,0:T(8,128)(2,1)} %param.23), kind=kOutput, calls=%fused_computation.31 | convolution fusion | flops 504913920 | bytes 4489216 | tf_op jit(solution)/shard_map/dot_general | solution.py:63
  97.4 0.7 fusion.5
  98.1 0.6 copy-done.7
  98.8 2.0 add_convert_fusion
  100.8 30.5 %reduce-scatter.3.cloned.1.call-done = bf16[480,512]{1,0:T(8,128)(2,1)} async-done(((bf16[480,2048]{1,0:T(8,128)(2,1)}), bf16[480,512]{1,0:T(8,128)(2,1)}) %reduce-scatter.3.cloned.1.call-update) | async-done | bytes 491536 | tf_op jit(solution)/shard_map/reduce_scatter | solution.py:135
  131.3 1.1 reshape.140
  132.4 19.7 %all_to_all.17 = bf16[8,60,512]{2,1,0:T(8,128)(2,1)S(1)} all-to-all(bf16[8,60,512]{2,1,0:T(8,128)(2,1)S(1)} %reshape.140), channel_id=1, replica_groups=mesh['sp'=8,'tp'=4] {'sp'}, dimensions={0} | all-to-all | bytes 983040 | tf_op jit(solution)/shard_map/all_to_all | solution.py:138
  152.1 8.6 %collective-permute-done = bf16[8,60,512]{2,1,0:T(8,128)(2,1)S(1)} collective-permute-done((bf16[8,60,512]{2,1,0:T(8,128)(2,1)S(1)}, bf16[8,60,512]{2,1,0:T(8,128)(2,1)S(1)}, u32[]{:S(2)}, u32[]{:S(2)}) %collective-permute-start) | collective-permute-done | bytes 491552 | tf_op jit(solution)/shard_map/ppermute | solution.py:16
  160.7 8.6 %collective-permute-done.1 = bf16[8,60,512]{2,1,0:T(8,128)(2,1)S(1)} collective-permute-done((bf16[8,60,512]{2,1,0:T(8,128)(2,1)S(1)}, bf16[8,60,512]{2,1,0:T(8,128)(2,1)S(1)}, u32[]{:S(2)}, u32[]{:S(2)}) %collective-permute-start.1) | collective-permute-done | bytes 491552 | tf_op jit(solution)/shard_map/ppermute | solution.py:16
  169.3 0.2 fusion.19
  169.5 9.4 %all-reduce.3 = (f32[192]{0:T(256)S(1)}, f32[192]{0:T(256)S(1)}) all-reduce(f32[192]{0:T(256)S(1)} %get-tuple-element.9, f32[192]{0:T(256)S(1)} %get-tuple-element.8), channel_id=1, replica_groups=mesh['sp'=8,'tp'=4] {'tp'}, use_global_device_ids=true, to_apply=%region_3.4 | all-reduce | flops 384 | bytes 3072 | tf_op jit(solution)/shard_map/psum | solution.py:158
  179.2 0.1 constant_dynamic-update-slice_fusion.3
  179.5 1.6 constant_dynamic-slice_fusion
  181.1 1.7 reshape.141
  182.8 3.1 %gather_fusion.2 = bf16[384,2048]{1,0:T(8,128)(2,1)} fusion(bf16[480,2048]{1,0:T(8,128)(2,1)S(1)} %reshape.141, s32[1024]{0:T(1024)S(1)} %pad_clamp_fusion), kind=kCustom, calls=%fused_computation.2 | custom fusion | bytes 3147264 | tf_op jit(solution)/shard_map/gather | solution.py:146
  186.0 4.7 %reshape.142 = f32[192,2,2048]{2,1,0:T(2,128)} reshape(bf16[384,2048]{1,0:T(8,128)(2,1)} %gather_fusion.2) | data formatting | bytes 4718592 | tf_op jit(solution)/shard_map/convert_element_type | solution.py:146
  190.7 6.1 %fusion.62 = (f32[192,1,2048]{2,1,0:T(1,128)S(1)}, f32[192,1,2048]{2,1,0:T(1,128)S(1)}) fusion(f32[192,2,2048]{2,1,0:T(2,128)} %reshape.142), kind=kLoop, calls=%fused_computation.121 | loop fusion | bytes 6291456 | tf_op jit(solution)/shard_map/slice | solution.py:147
  196.9 1.0 fusion.1
  197.9 0.1 copy-done.5
  198.0 1.9 subtract_convert_fusion
  199.9 1.9 fusion.42
  201.8 0.1 rev.3
  202.0 3.8 %convolution_bitcast_fusion.1 = f32[1,2048,256]{2,1,0:T(8,128)} fusion(bf16[480,2048]{1,0:T(8,128)(2,1)} %copy-done.6, bf16[480,256]{1,0:T(8,128)(2,1)S(1)} %copy-done.13), kind=kOutput, calls=%fused_computation.6 | convolution fusion | flops 503316480 | bytes 4308992 | tf_op jit(solution)/shard_map/dot_general | solution.py:69
  205.8 2.1 convolution_bitcast_fusion
  207.9 0.6 fusion.61
  208.5 6.2 %all-reduce.2 = (f32[192]{0:T(256)S(1)}, f32[192]{0:T(256)S(1)}) all-reduce(f32[192]{0:T(256)S(1)} %get-tuple-element.7, f32[192]{0:T(256)S(1)} %get-tuple-element.6), channel_id=1, replica_groups=mesh['sp'=8,'tp'=4] {'tp'}, use_global_device_ids=true, to_apply=%region_14.15 | all-reduce | flops 384 | bytes 3072 | tf_op jit(solution)/shard_map/psum | solution.py:167
  214.8 0.2 fusion.37
  215.0 1.3 collective-permute-start.3
  216.3 3.7 %convolution_bitcast_fusion.2 = f32[1,2048,256]{2,1,0:T(8,128)} fusion(bf16[480,2048]{1,0:T(8,128)(2,1)} %copy-done.6, bf16[480,256]{1,0:T(8,128)(2,1)S(1)} %copy-done.15), kind=kOutput, calls=%fused_computation.7 | convolution fusion | flops 503316480 | bytes 4308992 | tf_op jit(solution)/shard_map/dot_general | solution.py:69
  219.9 0.8 collective-permute-done.3
  220.8 2.9 %fusion.17 = f32[1,192,256]{2,0,1:T(1,128)S(1)} fusion(bf16[1,222,256]{2,1,0:T(8,128)(2,1)S(1)} %maximum_bitcast_fusion, f32[31,1,256]{2,0,1:T(8,128)S(1)} %bitcast.71), kind=kOutput, calls=%fused_computation.40 | convolution fusion | flops 18284544 | bytes 342016 | tf_op jit(solution)/shard_map/conv_general_dilated | solution.py:177
  223.7 0.8 fusion.41
  224.4 44.0 %reduce-scatter.5.cloned.1.call-done = f32[256,256]{1,0:T(8,128)} async-done(((f32[2048,256]{1,0:T(8,128)}), f32[256,256]{1,0:T(8,128)}) %reduce-scatter.5.cloned.1.call-update) | async-done | bytes 262160 | tf_op jit(solution)/shard_map/reduce_scatter | solution.py:191
  (86 shorter events, 1.1 us)
Async XLA Ops:
  7.2 68.3 %copy-start = (bf16[1,2048,256]{2,1,0:T(8,128)(2,1)S(1)}, bf16[1,2048,256]{2,1,0:T(8,128)(2,1)}, u32[]{:S(2)}) copy-start(bf16[1,2048,256]{2,1,0:T(8,128)(2,1)} %param.21) | copy-start | bytes 3145732
  7.2 9.1 %copy-start.18 = (f32[2048]{0:T(1024)S(1)}, f32[2048]{0:T(1024)}, u32[]{:S(2)}) copy-start(f32[2048]{0:T(1024)} %param.17) | copy-start | bytes 24580
  7.2 63.8 %all-gather.5.cloned.1.call-start = ((), (), s32[]{:S(2)}) async-start(), calls=%async_computation.6 | async-start | bytes 2621440 | tf_op jit(solution)/shard_map/all_gather | solution.py:118
  18.6 22.1 %copy-start.20 = (f32[192,2]{0,1:T(2,128)S(1)}, f32[192,2]{0,1:T(2,128)}, u32[]{:S(2)}) copy-start(f32[192,2]{0,1:T(2,128)} %param.20) | copy-start | bytes 4612
  18.6 22.4 %copy-start.21 = (f32[192]{0:T(256)S(1)}, f32[192]{0:T(256)}, u32[]{:S(2)}) copy-start(f32[192]{0:T(256)} %param.19) | copy-start | bytes 2308
  18.6 22.6 %copy-start.4 = (bf16[192,2048]{1,0:T(8,128)(2,1)S(1)}, bf16[192,2048]{1,0:T(8,128)(2,1)}, u32[]{:S(2)}) copy-start(bf16[192,2048]{1,0:T(8,128)(2,1)} %param.16) | copy-start | bytes 2359300
  40.6 52.1 %all-gather.3.cloned.1.call-start = ((), (), s32[]{:S(2)}) async-start(), calls=%async_computation.5 | async-start | bytes 2621440 | tf_op jit(solution)/shard_map/all_gather | solution.py:119
  71.0 60.4 %reduce-scatter.3.cloned.1.call-start = ((), (), s32[]{:S(2)}) async-start(), calls=%async_computation.7 | async-start | bytes 2457600 | tf_op jit(solution)/shard_map/reduce_scatter | solution.py:135
  72.8 4.1 %copy-start.6 = (bf16[480,2048]{1,0:T(8,128)(2,1)}, bf16[480,2048]{1,0:T(8,128)(2,1)S(1)}, u32[]{:S(2)}) copy-start(bf16[480,2048]{1,0:T(8,128)(2,1)S(1)} %reshape.139) | copy-start | bytes 5898244
  75.4 19.1 %copy-start.9 = (f32[480,256]{1,0:T(8,128)}, f32[480,256]{1,0:T(8,128)S(1)}, u32[]{:S(2)}) copy-start(f32[480,256]{1,0:T(8,128)S(1)} %fusion.10) | copy-start | bytes 1474564
  94.5 2.8 %copy-start.2 = (bf16[480,2048]{1,0:T(8,128)(2,1)}, bf16[480,2048]{1,0:T(8,128)(2,1)S(1)}, u32[]{:S(2)}) copy-start(bf16[480,2048]{1,0:T(8,128)(2,1)S(1)} %reshape.137) | copy-start | bytes 5898244
  97.4 0.8 copy-start.14
  97.4 0.8 copy-start.12
  97.4 1.4 copy-start.7
  100.8 68.6 %copy-start.8 = (bf16[192,256]{1,0:T(8,128)(2,1)S(1)}, bf16[192,256]{1,0:T(8,128)(2,1)}, u32[]{:S(2)}) copy-start(bf16[192,256]{1,0:T(8,128)(2,1)} %param.25) | copy-start | bytes 294916
  100.8 167.6 %reduce-scatter.5.cloned.1.call-start = ((), (), s32[]{:S(2)}) async-start(), calls=%async_computation.8 | async-start | bytes 2359296 | tf_op jit(solution)/shard_map/reduce_scatter | solution.py:191
  152.1 8.6 %collective-permute-start = (bf16[8,60,512]{2,1,0:T(8,128)(2,1)S(1)}, bf16[8,60,512]{2,1,0:T(8,128)(2,1)S(1)}, u32[]{:S(2)}, u32[]{:S(2)}) collective-permute-start(bf16[8,60,512]{2,1,0:T(8,128)(2,1)S(1)} %all_to_all.17), channel_id=1, source_target_pairs={{0,1},{1,2},{2,3},{3,0},{4,5},{5,6},{6,7},{7,4},{8,9},{9,10},{10,1... | collective-permute-start | bytes 1474568 | tf_op jit(solution)/shard_map/ppermute | solution.py:16
  160.7 8.6 %collective-permute-start.1 = (bf16[8,60,512]{2,1,0:T(8,128)(2,1)S(1)}, bf16[8,60,512]{2,1,0:T(8,128)(2,1)S(1)}, u32[]{:S(2)}, u32[]{:S(2)}) collective-permute-start(bf16[8,60,512]{2,1,0:T(8,128)(2,1)S(1)} %collective-permute-done), channel_id=1, source_target_pairs={{0,1},{1,2},{2,3},{3,0},{4,5},{5,6},{6,7},{7,4},{8,9},{9,10},{10,1... | collective-permute-start | bytes 1474568 | tf_op jit(solution)/shard_map/ppermute | solution.py:16
  169.3 9.6 %collective-permute-start.2 = (bf16[8,60,512]{2,1,0:T(8,128)(2,1)S(1)}, bf16[8,60,512]{2,1,0:T(8,128)(2,1)S(1)}, u32[]{:S(2)}, u32[]{:S(2)}) collective-permute-start(bf16[8,60,512]{2,1,0:T(8,128)(2,1)S(1)} %collective-permute-done.1), channel_id=1, source_target_pairs={{0,1},{1,2},{2,3},{3,0},{4,5},{5,6},{6,7},{7,4},{8,9},{9,10},{10,1... | collective-permute-start | bytes 1474568 | tf_op jit(solution)/shard_map/ppermute | solution.py:16
  190.7 6.1 %copy-start.1 = (bf16[192,2048]{1,0:T(8,128)(2,1)S(1)}, bf16[192,2048]{1,0:T(8,128)(2,1)}, u32[]{:S(2)}) copy-start(bf16[192,2048]{1,0:T(8,128)(2,1)} %param.15) | copy-start | bytes 2359300
  196.8 1.1 copy-start.5
  198.0 1.9 copy-start.22
  199.9 2.0 copy-start.19
  199.9 2.0 copy-start.13
  201.9 3.8 %copy-start.3 = (bf16[480,2048]{1,0:T(8,128)(2,1)S(1)}, bf16[480,2048]{1,0:T(8,128)(2,1)}, u32[]{:S(2)}) copy-start(bf16[480,2048]{1,0:T(8,128)(2,1)} %copy-done.2) | copy-start | bytes 5898244
  201.9 3.8 %copy-start.10 = (f32[480,256]{1,0:T(8,128)S(1)}, f32[480,256]{1,0:T(8,128)}, u32[]{:S(2)}) copy-start(f32[480,256]{1,0:T(8,128)} %copy-done.9) | copy-start | bytes 1474564
  201.9 3.8 %copy-start.11 = (f32[480,256]{1,0:T(8,128)S(1)}, f32[480,256]{1,0:T(8,128)}, u32[]{:S(2)}) copy-start(f32[480,256]{1,0:T(8,128)} %fusion.7) | copy-start | bytes 1474564
  205.8 2.1 copy-start.23
  207.9 8.4 %copy-start.15 = (bf16[480,256]{1,0:T(8,128)(2,1)S(1)}, bf16[480,256]{1,0:T(8,128)(2,1)}, u32[]{:S(2)}) copy-start(bf16[480,256]{1,0:T(8,128)(2,1)} %copy-done.14) | copy-start | bytes 737284
  215.0 5.8 %collective-permute-start.3 = (bf16[30,256]{1,0:T(8,128)(2,1)S(1)}, bf16[30,256]{1,0:T(8,128)(2,1)S(1)}, u32[]{:S(2)}, u32[]{:S(2)}) collective-permute-start(bf16[30,256]{1,0:T(8,128)(2,1)S(1)} %slice.37), channel_id=1, source_target_pairs={{4,0},{8,4},{12,8},{16,12},{20,16},{24,20},{28,24},{5,1},{9,5},{13... | collective-permute-start | bytes 46088 | tf_op jit(solution)/shard_map/ppermute | solution.py:29
  220.7 2.9 %copy-start.16 = (bf16[192,256]{1,0:T(8,128)(2,1)S(1)}, bf16[192,256]{1,0:T(8,128)(2,1)}, u32[]{:S(2)}) copy-start(bf16[192,256]{1,0:T(8,128)(2,1)} %param.28) | copy-start | bytes 294916
  220.8 2.9 %copy-start.17 = (bf16[192,256]{1,0:T(8,128)(2,1)S(1)}, bf16[192,256]{1,0:T(8,128)(2,1)}, u32[]{:S(2)}) copy-start(bf16[192,256]{1,0:T(8,128)(2,1)} %param.29) | copy-start | bytes 294916
Sparse Core Ops, SparseCore 0:
  40.7 21.5 all-gather.4
  71.1 21.6 all-gather.2
  100.9 30.3 reduce-scatter.2
  201.9 66.4 reduce-scatter.4
